TPU v7x, 32 devices: a whole 2x2x4 slice. The times are simulated.
32 devices in a mesh: fs: 8 (over z, y), tp: 4 (over x, core).
Axes of the slice: x: 2, y: 2, z: 4, core: 2. Of those that a mesh axis runs over, the one named last changes fastest.
Arguments:
- late_input: bfloat16 [2048, 2048], P(('fs', 'tp')), may hold values from -6 to 6
- early_input: bfloat16 [2048, 2048], P(('fs', 'tp')), may hold values from -6 to 6
- early_grad: bfloat16 [2048, 2048], P(('fs', 'tp')), may hold values from -6 to 6
- pre_gain: float32 [2048], replicated, may hold values from 0.1 to 1.9
- post_gain: float32 [2048], replicated, may hold values from 0.1 to 1.9
- gate_weight: bfloat16 [2048, 4096], P('fs', 'tp'), may hold values from -0.125 to 0.125
- up_weight: bfloat16 [2048, 4096], P('fs', 'tp'), may hold values from -0.125 to 0.125
- down_weight: bfloat16 [2048, 4096], P('fs', 'tp'), may hold values from -0.09375 to 0.09375
- gate_sum: float32 [2048, 4096], P('fs', 'tp'), may hold values from -1.8 to 1.8
- up_sum: float32 [2048, 4096], P('fs', 'tp'), may hold values from -1.8 to 1.8
- down_gradient_sum: float32 [2048, 4096], P('fs', 'tp'), may hold values from -1.8 to 1.8
Outputs:
- late_output: bfloat16 [2048, 2048], P(('fs', 'tp'))
- early_input_grad: bfloat16 [2048, 2048], P(('fs', 'tp'))
- gate_total: float32 [2048, 4096], P('fs', 'tp')
- up_total: float32 [2048, 4096], P('fs', 'tp')
- down_total: float32 [2048, 4096], P('fs', 'tp')
All inputs are finite; a program needn't handle non-finite values.
Results may differ from a plain program's by a relative error of at most 0.013.
Values may be sent and summed in bfloat16 or wider, within the bound.
A program may use at most 128 MiB of HBM per device.

v0:
```python
import math
import jax
import jax.numpy as jnp
from jax import lax
from jax.sharding import PartitionSpec as P

NORM_EPS = 1e-06


def contract_last(first_op, second_op):
    return lax.dot_general(
        first_op, second_op, (((1,), (1,)), ((), ())), preferred_element_type=jnp.float32
    )


def contract_first(first_op, second_op):
    return lax.dot_general(
        first_op, second_op, (((0,), (0,)), ((), ())), preferred_element_type=jnp.float32
    )


def inverse_rms(values):
    return lax.rsqrt(jnp.mean(values * values, axis=-1, keepdims=True) + NORM_EPS)


def per_device(
    late_input,
    early_input,
    early_grad,
    pre_gain,
    post_gain,
    gate_weight,
    up_weight,
    down_weight,
    gate_sum,
    up_sum,
    down_gradient_sum,
):
    tok_rows, model_width = late_input.shape
    group_rows = tok_rows * lax.axis_size("tp")
    grad_scale = 1.0 / math.sqrt(group_rows * lax.axis_size("fs"))
    hidden_width = gate_sum.shape[1]
    input_rows = jnp.stack([late_input, early_input]).astype(jnp.float32)
    input_inverse = inverse_rms(input_rows)
    normed = (input_rows * input_inverse * pre_gain).astype(jnp.bfloat16)
    normed_rows = lax.all_gather(normed, "tp", axis=1, tiled=True)
    gate_all, up_all, down_gradient_rows = (
        lax.all_gather(gate_weight, "fs", axis=0, tiled=True),
        lax.all_gather(up_weight, "fs", axis=0, tiled=True),
        lax.all_gather(down_weight, "fs", axis=0, tiled=True),
    )
    flat_rows = normed_rows.reshape(2 * group_rows, model_width)
    gate_pre = jnp.dot(flat_rows, gate_all, preferred_element_type=jnp.float32)
    up_pre = jnp.dot(flat_rows, up_all, preferred_element_type=jnp.float32)
    hidden_state = (
        (jax.nn.silu(gate_pre) * up_pre).astype(jnp.bfloat16).reshape(2, group_rows, hidden_width)
    )
    gated_product = jnp.einsum(
        "utx,ix->tui", hidden_state, down_gradient_rows, preferred_element_type=jnp.float32
    )
    mixed_sum = lax.psum_scatter(
        gated_product.reshape(lax.axis_size("tp") * tok_rows, 2 * model_width).astype(jnp.bfloat16),
        "tp",
        scatter_dimension=0,
        tiled=True,
    ).astype(jnp.float32)
    mixed_sum = lax.optimization_barrier(mixed_sum.astype(jnp.bfloat16)).astype(jnp.float32)
    mixed_sum = mixed_sum.reshape(tok_rows, 2, model_width)
    mixed_inverse = inverse_rms(mixed_sum)
    late_output = (input_rows[0] + 0.5 * mixed_sum[:, 0] * mixed_inverse[:, 0] * post_gain).astype(
        jnp.bfloat16
    )
    early_mixed = mixed_sum[:, 1]
    early_inverse_norm = mixed_inverse[:, 1]
    weighted = 0.5 * early_grad.astype(jnp.float32) * post_gain
    mixed_cot = (
        early_inverse_norm * weighted
        - early_mixed
        * early_inverse_norm**3
        * jnp.mean(weighted * early_mixed, axis=-1, keepdims=True)
    ).astype(jnp.bfloat16)
    cot_rows = lax.all_gather(mixed_cot, "tp", axis=0, tiled=True)
    early_hidden = hidden_state[1]
    early_normed = normed_rows[1]
    hidden_cot = jnp.dot(cot_rows, down_gradient_rows, preferred_element_type=jnp.float32)
    early_gate = gate_pre[group_rows:]
    early_up = up_pre[group_rows:]
    sigmoid_gate = jax.nn.sigmoid(early_gate)
    gate_cot = (
        hidden_cot * early_up * sigmoid_gate * (1.0 + early_gate * (1.0 - sigmoid_gate))
    ).astype(jnp.bfloat16)
    up_cot = (hidden_cot * early_gate * sigmoid_gate).astype(jnp.bfloat16)
    normed_cot = lax.psum_scatter(
        (contract_last(gate_cot, gate_all) + contract_last(up_cot, up_all)).astype(jnp.bfloat16),
        "tp",
        scatter_dimension=0,
        tiled=True,
    ).astype(jnp.float32)
    normed_cot = lax.optimization_barrier(normed_cot.astype(jnp.bfloat16)).astype(jnp.float32)
    weighted_in = normed_cot * pre_gain
    early_values = input_rows[1]
    early_in_inverse = input_inverse[1]
    early_input_grad = (
        early_grad.astype(jnp.float32)
        + early_in_inverse * weighted_in
        - early_values
        * early_in_inverse**3
        * jnp.mean(weighted_in * early_values, axis=-1, keepdims=True)
    ).astype(jnp.bfloat16)
    totals = lax.psum_scatter(
        (
            grad_scale
            * jnp.concatenate(
                [
                    contract_first(early_normed, gate_cot),
                    contract_first(early_normed, up_cot),
                    contract_first(cot_rows, early_hidden),
                ],
                1,
            )
        ).astype(jnp.bfloat16),
        "fs",
        scatter_dimension=0,
        tiled=True,
    ).astype(jnp.float32)
    gate_total = gate_sum + totals[:, :hidden_width]
    up_total = up_sum + totals[:, hidden_width : 2 * hidden_width]
    down_total = down_gradient_sum + totals[:, 2 * hidden_width :]
    return (late_output, early_input_grad, gate_total, up_total, down_total)


def solution(mesh):
    in_specs = (
        P(("fs", "tp"), None),
        P(("fs", "tp"), None),
        P(("fs", "tp"), None),
        P(),
        P(),
        P("fs", "tp"),
        P("fs", "tp"),
        P("fs", "tp"),
        P("fs", "tp"),
        P("fs", "tp"),
        P("fs", "tp"),
    )
    out_specs = (
        P(("fs", "tp"), None),
        P(("fs", "tp"), None),
        P("fs", "tp"),
        P("fs", "tp"),
        P("fs", "tp"),
    )
    return jax.shard_map(
        per_device, mesh=mesh, in_specs=in_specs, out_specs=out_specs, check_vma=False
    )
```

profile of v0, /device:TPU:0, one launch (start us, length us, event | category | flops | bytes accessed | tf_op | source)
XLA Modules:
  0.0 585.3 jit_solution(17200032101775942609)
XLA Ops:
  7.2 1.2 multiply_reduce_fusion.1
  8.4 2.0 multiply_convert_fusion.2
  12.6 23.3 %all-gather.6.cloned.1.call-done = bf16[2,256,2048]{2,1,0:T(8,128)(2,1)} async-done(((bf16[2,64,2048]{2,1,0:T(8,128)(2,1)}), bf16[2,256,2048]{2,1,0:T(8,128)(2,1)}) %all-gather.6.cloned.1.call-update) | async-done | bytes 2097168 | tf_op jit(solution)/shard_map/all_gather | solution.py:46
  35.9 75.0 %all-gather.8.cloned.1.call-done = bf16[2048,1024]{1,0:T(8,128)(2,1)} async-done(((bf16[256,1024]{1,0:T(8,128)(2,1)}), bf16[2048,1024]{1,0:T(8,128)(2,1)}) %all-gather.8.cloned.1.call-update) | async-done | bytes 4194320 | tf_op jit(solution)/shard_map/all_gather | solution.py:48
  110.9 6.6 %fusion.29 = f32[512,1024]{1,0:T(8,128)} fusion(bf16[512,2048]{1,0:T(8,128)(2,1)} %bitcast.71, bf16[2048,1024]{1,0:T(8,128)(2,1)} %all-gather.8.cloned.1.call-done), kind=kOutput, calls=%fused_computation.57 | convolution fusion | flops 2147483648 | bytes 8388608 | tf_op jit(solution)/shard_map/dot_general | solution.py:53
  117.5 66.9 %all-gather.10.cloned.1.call-done = bf16[2048,1024]{1,0:T(8,128)(2,1)} async-done(((bf16[256,1024]{1,0:T(8,128)(2,1)}), bf16[2048,1024]{1,0:T(8,128)(2,1)}) %all-gather.10.cloned.1.call-update) | async-done | bytes 4194320 | tf_op jit(solution)/shard_map/all_gather | solution.py:49
  184.4 6.6 %multiply_convert_fusion = (bf16[512,1024]{1,0:T(8,128)(2,1)S(1)}, f32[512,1024]{1,0:T(8,128)}) fusion(f32[512,1024]{1,0:T(8,128)} %fusion.29, bf16[512,2048]{1,0:T(8,128)(2,1)S(1)} %bitcast.72, bf16[2048,1024]{1,0:T(8,128)(2,1)} %all-gather.10.cloned.1.call-done), kind=kOutput, calls=%fused_computation.8 | convolution fusion | flops 2150629376 | bytes 11534336 | tf_op jit(solution)/shard_map/dot_general | solution.py:54
  191.0 66.8 %all-gather.12.cloned.1.call-done = bf16[2048,1024]{1,0:T(8,128)(2,1)} async-done(((bf16[256,1024]{1,0:T(8,128)(2,1)}), bf16[2048,1024]{1,0:T(8,128)(2,1)}) %all-gather.12.cloned.1.call-update) | async-done | bytes 4194320 | tf_op jit(solution)/shard_map/all_gather | solution.py:50
  257.7 5.9 %fusion.6 = bf16[256,2,2048]{2,0,1:T(8,128)(2,1)} fusion(bf16[2,256,1024]{2,1,0:T(8,128)(2,1)S(1)} %bitcast.79, bf16[2048,1024]{1,0:T(8,128)(2,1)} %all-gather.12.cloned.1.call-done), kind=kOutput, calls=%fused_computation.5 | convolution fusion | flops 2148532224 | bytes 7340032 | tf_op jit(solution)/shard_map/utx,ix->tui/dot_general | solution.py:58
  263.6 2.8 copy.43
  266.4 2.9 copy.54
  269.5 29.8 %reduce-scatter.10.cloned.1.call-done = bf16[64,4096]{1,0:T(8,128)(2,1)} async-done(((bf16[256,4096]{1,0:T(8,128)(2,1)}), bf16[64,4096]{1,0:T(8,128)(2,1)}) %reduce-scatter.10.cloned.1.call-update) | async-done | bytes 524304
  299.2 1.5 copy.55
  302.1 1.6 fusion.28
  305.8 16.6 %all-gather.14.cloned.1.call-done = bf16[256,2048]{1,0:T(8,128)(2,1)} async-done(((bf16[64,2048]{1,0:T(8,128)(2,1)}), bf16[256,2048]{1,0:T(8,128)(2,1)}) %all-gather.14.cloned.1.call-update) | async-done | bytes 1048592 | tf_op jit(solution)/shard_map/all_gather | solution.py:82
  322.5 4.7 multiply_convert_fusion.1
  327.3 1.3 fusion.30
  328.6 1.2 copy-done.16
  329.8 2.3 fusion.9
  332.2 2.5 fusion.22
  334.7 1.3 fusion.13
  336.0 1.3 fusion.14
  337.3 7.5 %fusion = bf16[2048,3072]{0,1:T(8,128)(2,1)} fusion(f32[2048,1024]{0,1:T(8,128)S(1)} %fusion.22, f32[2048,1024]{0,1:T(8,128)S(1)} %fusion.13, f32[2048,1024]{0,1:T(8,128)S(1)} %fusion.14), kind=kLoop, calls=%fused_computation.1 | loop fusion | flops 25165824 | bytes 37748736 | tf_op jit(solution)/shard_map/convert_element_type | solution.py:121
  346.8 2.5 copy.48
  350.4 6.6 %reduce-scatter.6.cloned.1.call-done = bf16[64,2048]{1,0:T(8,128)(2,1)} async-done(((bf16[256,2048]{1,0:T(8,128)(2,1)}), bf16[64,2048]{1,0:T(8,128)(2,1)}) %reduce-scatter.6.cloned.1.call-update) | async-done | bytes 262160 | tf_op jit(solution)/shard_map/reduce_scatter | solution.py:93
  358.2 2.2 fusion.21
  360.4 208.1 %reduce-scatter.8.cloned.1.call-done = bf16[256,3072]{0,1:T(8,128)(2,1)} async-done(((bf16[2048,3072]{0,1:T(8,128)(2,1)}), bf16[256,3072]{0,1:T(8,128)(2,1)}) %reduce-scatter.8.cloned.1.call-update) | async-done | bytes 1572880 | tf_op jit(solution)/shard_map/reduce_scatter | solution.py:110
  568.5 1.6 convert_element_type.69
  570.2 1.8 slice_add_fusion
  572.0 2.6 copy.51
  574.6 2.5 copy.52
  577.2 1.3 copy.53
  (67 shorter events, 9.9 us)
Async XLA Ops:
  7.2 28.8 %all-gather.6.cloned.1.call-start = ((), (), s32[]{:S(2)}) async-start(), calls=%async_computation.3 | async-start | bytes 2621440 | tf_op jit(solution)/shard_map/all_gather | solution.py:46
  10.5 100.4 %all-gather.8.cloned.1.call-start = ((), (), s32[]{:S(2)}) async-start(), calls=%async_computation.4 | async-start | bytes 4718592 | tf_op jit(solution)/shard_map/all_gather | solution.py:48
  11.2 173.1 %all-gather.10.cloned.1.call-start = ((), (), s32[]{:S(2)}) async-start(), calls=%async_computation.5 | async-start | bytes 4718592 | tf_op jit(solution)/shard_map/all_gather | solution.py:49
  12.0 245.7 %all-gather.12.cloned.1.call-start = ((), (), s32[]{:S(2)}) async-start(), calls=%async_computation.6 | async-start | bytes 4718592 | tf_op jit(solution)/shard_map/all_gather | solution.py:50
  12.6 286.7 %reduce-scatter.10.cloned.1.call-start = ((), (), s32[]{:S(2)}) async-start(), calls=%async_computation.10 | async-start | bytes 2621440
  110.9 73.5 %copy-start.2 = (bf16[2,256,2048]{2,1,0:T(8,128)(2,1)S(1)}, bf16[2,256,2048]{2,1,0:T(8,128)(2,1)}, u32[]{:S(2)}) copy-start(bf16[2,256,2048]{2,1,0:T(8,128)(2,1)} %all-gather.6.cloned.1.call-done) | copy-start | bytes 6291460
  190.9 72.6 %copy-start.12 = (bf16[512,1024]{1,0:T(8,128)(2,1)}, bf16[512,1024]{1,0:T(8,128)(2,1)S(1)}, u32[]{:S(2)}) copy-start(bf16[512,1024]{1,0:T(8,128)(2,1)S(1)} %get-tuple-element.36) | copy-start | bytes 3145732
  266.4 3.0 copy-start.14
  269.4 34.9 %copy-start.4 = (bf16[64,2048]{1,0:T(8,128)(2,1)S(1)}, bf16[64,2048]{1,0:T(8,128)(2,1)}, u32[]{:S(2)}) copy-start(bf16[64,2048]{1,0:T(8,128)(2,1)} %param.13) | copy-start | bytes 786436
  269.4 53.1 %all-gather.14.cloned.1.call-start = ((), (), s32[]{:S(2)}) async-start(), calls=%async_computation.7 | async-start | bytes 1310720 | tf_op jit(solution)/shard_map/all_gather | solution.py:82
  305.6 51.4 %reduce-scatter.6.cloned.1.call-start = ((), (), s32[]{:S(2)}) async-start(), calls=%async_computation.8 | async-start | bytes 1310720 | tf_op jit(solution)/shard_map/reduce_scatter | solution.py:93
  322.5 4.8 copy-start.15
  327.2 1.3 copy-start.8
  327.2 4.9 copy-start.10
  327.2 2.6 copy-start.16
  329.8 2.4 copy-start.5
  332.1 2.6 copy-start.3
  332.1 236.4 %reduce-scatter.8.cloned.1.call-start = ((), (), s32[]{:S(2)}) async-start(), calls=%async_computation.9 | async-start | bytes 14155776 | tf_op jit(solution)/shard_map/reduce_scatter | solution.py:110
  332.2 2.5 copy-start.11
  334.7 1.3 copy-start.9
  344.9 1.2 copy-start.6
  344.9 1.6 copy-start.7
  346.1 11.0 %copy-start.13 = (f32[2048]{0:T(1024)S(1)}, f32[2048]{0:T(1024)}, u32[]{:S(2)}) copy-start(f32[2048]{0:T(1024)} %param.14) | copy-start | bytes 24580
  360.4 209.8 %copy-start = (f32[256,1024]{0,1:T(8,128)S(1)}, f32[256,1024]{0,1:T(8,128)}, u32[]{:S(2)}) copy-start(f32[256,1024]{0,1:T(8,128)} %copy.48) | copy-start | bytes 3145732
  572.0 5.2 copy-start.1
Sparse Core Ops, SparseCore 0:
  10.6 25.2 all-gather.5
  38.1 72.7 all-gather.7
  113.0 71.3 all-gather.9
  186.4 71.3 all-gather.11
  269.5 29.6 reduce-scatter.9
  305.7 16.7 all-gather.13
  332.2 24.7 reduce-scatter.5
  360.7 207.8 reduce-scatter.7
where the time goes:
time: 586 us; the launch traced here: 585 us
  waiting for transfers between devices  495 us (84%)
  matrix products  32.4 us (6%)
  local copies, waits for them, and re-layouts  22.5 us (4%)
  other arithmetic  20.5 us (3%)
  between operations  14.4 us (2%)
    reduce_scatter x1, waiting for transfers between devices, per_device(): lax.psum_scatter((grad_scale * jnp.concatenate([contract_first(early_norm...  208 us
    all_gather x1, waiting for transfers between devices, per_device(): lax.all_gather(gate_weight, 'fs', axis=0, tiled=True)  75 us
    all_gather x1, waiting for transfers between devices, per_device(): lax.all_gather(up_weight, 'fs', axis=0, tiled=True)  66.9 us
    all_gather x1, waiting for transfers between devices, per_device(): lax.all_gather(down_weight, 'fs', axis=0, tiled=True)  66.8 us
    unnamed x9, waiting for transfers between devices  31.7 us
    all_gather x1, waiting for transfers between devices, per_device(): normed_rows = lax.all_gather(normed, 'tp', axis=1, tiled=True)  23.3 us
    unnamed x43, local copies, waits for them, and re-layouts  16.7 us
    all_gather x1, waiting for transfers between devices, per_device(): cot_rows = lax.all_gather(mixed_cot, 'tp', axis=0, tiled=True)  16.6 us
  transfers between devices with their start and end apart: 8, of which 8 were waited for; matrix products, arithmetic and copies ran while one was open for 6% of the time, Pallas kernels for 0%

commit v1 on v0

--- a/solution.py
+++ b/solution.py
@@ -45,7 +45,9 @@
     normed = (input_rows * input_inverse * pre_gain).astype(jnp.bfloat16)
     normed_rows = lax.all_gather(normed, "tp", axis=1, tiled=True)
     gate_all, up_all, down_gradient_rows = (
-        lax.all_gather(gate_weight, "fs", axis=0, tiled=True),
+        jnp.concatenate(
+            lax.all_to_all(jnp.stack([gate_weight] * lax.axis_size("fs")), "fs", 0, 0), axis=0
+        ),
         lax.all_gather(up_weight, "fs", axis=0, tiled=True),
         lax.all_gather(down_weight, "fs", axis=0, tiled=True),
     )

time: 586 us -> 565 us (0.964)
  waiting for transfers between devices: 495 us -> 462 us
  starting transfers between devices: 0.5 us -> 7.77 us
    all_to_all x0 -> x1, waiting for transfers between devices: none -> 130 us  [per_device(): lax.all_to_all(jnp.stack([gate_weight] * lax.axis_size('fs')), 'fs', 0, 0)]
    all_gather x1 -> x0, waiting for transfers between devices: 75 us -> none  [per_device(): lax.all_gather(gate_weight, 'fs', axis=0, tiled=True)]
    all_gather x1, waiting for transfers between devices: 66.9 us -> 0.01 us  [per_device(): lax.all_gather(up_weight, 'fs', axis=0, tiled=True)]
    all_gather x1, waiting for transfers between devices: 66.8 us -> 56.1 us  [per_device(): lax.all_gather(down_weight, 'fs', axis=0, tiled=True)]
    all_gather x1, waiting for transfers between devices: 23.3 us -> 13.1 us  [per_device(): normed_rows = lax.all_gather(normed, 'tp', axis=1, tiled=True)]
    all_to_all x0 -> x1, starting transfers between devices: none -> 7.31 us  [per_device(): lax.all_to_all(jnp.stack([gate_weight] * lax.axis_size('fs')), 'fs', 0, 0)]
    unnamed x43 -> x41, local copies, waits for them, and re-layouts: 16.7 us -> 15.5 us
    unnamed x9 -> x8, waiting for transfers between devices: 31.7 us -> 31.2 us
  transfers between devices with their start and end apart: 8 -> 8, of which waited for: 8 -> 7; matrix products, arithmetic and copies ran while one was open for 6% -> 7% of each run, Pallas kernels for 0% -> 0%
where the time goes in v1:
time: 565 us; the launch traced here: 564 us
  waiting for transfers between devices  462 us (82%)
  matrix products  34.9 us (6%)
  local copies, waits for them, and re-layouts  24.8 us (4%)
  other arithmetic  20.5 us (4%)
  between operations  14.4 us (3%)
  starting transfers between devices  7.77 us (1%)
    reduce_scatter x1, waiting for transfers between devices, per_device(): lax.psum_scatter((grad_scale * jnp.concatenate([contract_first(early_norm...  208 us
    all_to_all x1, waiting for transfers between devices, per_device(): lax.all_to_all(jnp.stack([gate_weight] * lax.axis_size('fs')), 'fs', 0, 0)  130 us
    all_gather x1, waiting for transfers between devices, per_device(): lax.all_gather(down_weight, 'fs', axis=0, tiled=True)  56.1 us
    unnamed x8, waiting for transfers between devices  31.2 us
    all_gather x1, waiting for transfers between devices, per_device(): cot_rows = lax.all_gather(mixed_cot, 'tp', axis=0, tiled=True)  16.6 us
    unnamed x41, local copies, waits for them, and re-layouts  15.5 us
    all_gather x1, waiting for transfers between devices, per_device(): normed_rows = lax.all_gather(normed, 'tp', axis=1, tiled=True)  13.1 us
  transfers between devices with their start and end apart: 8, of which 7 were waited for; matrix products, arithmetic and copies ran while one was open for 7% of the time, Pallas kernels for 0%

profile of v1, /device:TPU:0, one launch (start us, length us, event | category | flops | bytes accessed | tf_op | source)
XLA Modules:
  0.0 564.4 jit_solution(11139426827405601366)
XLA Ops:
  7.2 1.2 multiply_reduce_fusion.1
  8.4 2.0 multiply_convert_fusion.2
  11.2 3.5 stack.11
  14.8 7.3 %all-to-all-start = ((bf16[8,256,1024]{2,1,0:T(8,128)(2,1)}), bf16[8,256,1024]{2,1,0:T(8,128)(2,1)}, u32[]{:S(2)}, u32[]{:S(2)}) async-start(bf16[8,256,1024]{2,1,0:T(8,128)(2,1)} %stack.11), calls=%async_computation | async-start | bytes 8388608 | tf_op jit(solution)/shard_map/all_to_all | solution.py:49
  22.9 13.1 %all-gather.5.cloned.1.call-done = bf16[2,256,2048]{2,1,0:T(8,128)(2,1)} async-done(((bf16[2,64,2048]{2,1,0:T(8,128)(2,1)}), bf16[2,256,2048]{2,1,0:T(8,128)(2,1)}) %all-gather.5.cloned.1.call-update) | async-done | bytes 2097168 | tf_op jit(solution)/shard_map/all_gather | solution.py:46
  35.9 130.2 %all-to-all-done = bf16[8,256,1024]{2,1,0:T(8,128)(2,1)} async-done(((bf16[8,256,1024]{2,1,0:T(8,128)(2,1)}), bf16[8,256,1024]{2,1,0:T(8,128)(2,1)}, u32[]{:S(2)}, u32[]{:S(2)}) %all-to-all-start) | async-done | bytes 4194336 | tf_op jit(solution)/shard_map/all_to_all | solution.py:49
  166.1 6.6 %fusion.29 = f32[512,1024]{1,0:T(8,128)} fusion(bf16[512,2048]{1,0:T(8,128)(2,1)} %bitcast.72, bf16[2048,1024]{1,0:T(8,128)(2,1)} %bitcast.4), kind=kOutput, calls=%fused_computation.57 | convolution fusion | flops 2147483648 | bytes 8388608 | tf_op jit(solution)/shard_map/dot_general | solution.py:55
  172.8 6.6 %multiply_convert_fusion = (bf16[512,1024]{1,0:T(8,128)(2,1)S(1)}, f32[512,1024]{1,0:T(8,128)}) fusion(f32[512,1024]{1,0:T(8,128)} %fusion.29, bf16[512,2048]{1,0:T(8,128)(2,1)S(1)} %bitcast.73, bf16[2048,1024]{1,0:T(8,128)(2,1)} %all-gather.7.cloned.1.call-done), kind=kOutput, calls=%fused_computation.8 | convolution fusion | flops 2150629376 | bytes 11534336 | tf_op jit(solution)/shard_map/dot_general | solution.py:56
  179.3 56.1 %all-gather.9.cloned.1.call-done = bf16[2048,1024]{1,0:T(8,128)(2,1)} async-done(((bf16[256,1024]{1,0:T(8,128)(2,1)}), bf16[2048,1024]{1,0:T(8,128)(2,1)}) %all-gather.9.cloned.1.call-update) | async-done | bytes 4194320 | tf_op jit(solution)/shard_map/all_gather | solution.py:52
  235.4 5.9 %fusion.6 = bf16[256,2,2048]{2,0,1:T(8,128)(2,1)} fusion(bf16[2,256,1024]{2,1,0:T(8,128)(2,1)S(1)} %bitcast.80, bf16[2048,1024]{1,0:T(8,128)(2,1)} %all-gather.9.cloned.1.call-done), kind=kOutput, calls=%fused_computation.5 | convolution fusion | flops 2148532224 | bytes 7340032 | tf_op jit(solution)/shard_map/utx,ix->tui/dot_general | solution.py:60
  241.3 2.8 copy.43
  244.2 3.0 copy.54
  247.2 29.8 %reduce-scatter.10.cloned.1.call-done = bf16[64,4096]{1,0:T(8,128)(2,1)} async-done(((bf16[256,4096]{1,0:T(8,128)(2,1)}), bf16[64,4096]{1,0:T(8,128)(2,1)}) %reduce-scatter.10.cloned.1.call-update) | async-done | bytes 524304
  277.0 1.5 copy.55
  279.9 1.6 fusion.28
  283.6 16.6 %all-gather.11.cloned.1.call-done = bf16[256,2048]{1,0:T(8,128)(2,1)} async-done(((bf16[64,2048]{1,0:T(8,128)(2,1)}), bf16[256,2048]{1,0:T(8,128)(2,1)}) %all-gather.11.cloned.1.call-update) | async-done | bytes 1048592 | tf_op jit(solution)/shard_map/all_gather | solution.py:84
  300.2 4.6 multiply_convert_fusion.1
  304.8 3.9 fusion.30
  308.8 2.3 fusion.9
  311.2 2.5 fusion.22
  313.7 1.3 fusion.13
  315.0 1.3 fusion.14
  316.3 7.5 %fusion = bf16[2048,3072]{0,1:T(8,128)(2,1)} fusion(f32[2048,1024]{0,1:T(8,128)S(1)} %fusion.22, f32[2048,1024]{0,1:T(8,128)S(1)} %fusion.13, f32[2048,1024]{0,1:T(8,128)S(1)} %fusion.14), kind=kLoop, calls=%fused_computation.1 | loop fusion | flops 25165824 | bytes 37748736 | tf_op jit(solution)/shard_map/convert_element_type | solution.py:123
  325.8 2.5 copy.48
  329.4 6.7 %reduce-scatter.6.cloned.1.call-done = bf16[64,2048]{1,0:T(8,128)(2,1)} async-done(((bf16[256,2048]{1,0:T(8,128)(2,1)}), bf16[64,2048]{1,0:T(8,128)(2,1)}) %reduce-scatter.6.cloned.1.call-update) | async-done | bytes 262160 | tf_op jit(solution)/shard_map/reduce_scatter | solution.py:95
  337.2 2.2 fusion.21
  339.4 208.1 %reduce-scatter.8.cloned.1.call-done = bf16[256,3072]{0,1:T(8,128)(2,1)} async-done(((bf16[2048,3072]{0,1:T(8,128)(2,1)}), bf16[256,3072]{0,1:T(8,128)(2,1)}) %reduce-scatter.8.cloned.1.call-update) | async-done | bytes 1572880 | tf_op jit(solution)/shard_map/reduce_scatter | solution.py:112
  547.6 1.6 convert_element_type.69
  549.3 1.8 slice_add_fusion
  551.1 2.6 copy.51
  553.7 2.5 copy.52
  556.2 1.3 copy.53
  (65 shorter events, 9.3 us)
Async XLA Ops:
  7.2 28.8 %all-gather.5.cloned.1.call-start = ((), (), s32[]{:S(2)}) async-start(), calls=%async_computation.4 | async-start | bytes 2621440 | tf_op jit(solution)/shard_map/all_gather | solution.py:46
  10.5 162.3 %all-gather.7.cloned.1.call-start = ((), (), s32[]{:S(2)}) async-start(), calls=%async_computation.5 | async-start | bytes 4718592 | tf_op jit(solution)/shard_map/all_gather | solution.py:51
  14.8 151.4 %all-to-all-start = ((bf16[8,256,1024]{2,1,0:T(8,128)(2,1)}), bf16[8,256,1024]{2,1,0:T(8,128)(2,1)}, u32[]{:S(2)}, u32[]{:S(2)}) async-start(bf16[8,256,1024]{2,1,0:T(8,128)(2,1)} %stack.11), calls=%async_computation | async-start | bytes 8388608 | tf_op jit(solution)/shard_map/all_to_all | solution.py:49
  22.1 213.3 %all-gather.9.cloned.1.call-start = ((), (), s32[]{:S(2)}) async-start(), calls=%async_computation.6 | async-start | bytes 4718592 | tf_op jit(solution)/shard_map/all_gather | solution.py:52
  22.8 254.2 %reduce-scatter.10.cloned.1.call-start = ((), (), s32[]{:S(2)}) async-start(), calls=%async_computation.10 | async-start | bytes 2621440
  166.1 6.6 %copy-start.2 = (bf16[2,256,2048]{2,1,0:T(8,128)(2,1)S(1)}, bf16[2,256,2048]{2,1,0:T(8,128)(2,1)}, u32[]{:S(2)}) copy-start(bf16[2,256,2048]{2,1,0:T(8,128)(2,1)} %all-gather.5.cloned.1.call-done) | copy-start | bytes 6291460
  179.3 62.0 %copy-start.12 = (bf16[512,1024]{1,0:T(8,128)(2,1)}, bf16[512,1024]{1,0:T(8,128)(2,1)S(1)}, u32[]{:S(2)}) copy-start(bf16[512,1024]{1,0:T(8,128)(2,1)S(1)} %get-tuple-element.36) | copy-start | bytes 3145732
  244.2 3.1 copy-start.14
  247.1 34.9 %copy-start.4 = (bf16[64,2048]{1,0:T(8,128)(2,1)S(1)}, bf16[64,2048]{1,0:T(8,128)(2,1)}, u32[]{:S(2)}) copy-start(bf16[64,2048]{1,0:T(8,128)(2,1)} %param.13) | copy-start | bytes 786436
  247.2 53.1 %all-gather.11.cloned.1.call-start = ((), (), s32[]{:S(2)}) async-start(), calls=%async_computation.7 | async-start | bytes 1310720 | tf_op jit(solution)/shard_map/all_gather | solution.py:84
  283.4 52.7 %reduce-scatter.6.cloned.1.call-start = ((), (), s32[]{:S(2)}) async-start(), calls=%async_computation.8 | async-start | bytes 1310720 | tf_op jit(solution)/shard_map/reduce_scatter | solution.py:95
  304.8 4.0 copy-start.8
  304.8 6.3 %copy-start.10 = (bf16[256,1024]{1,0:T(8,128)(2,1)}, bf16[256,1024]{1,0:T(8,128)(2,1)S(1)}, u32[]{:S(2)}) copy-start(bf16[256,1024]{1,0:T(8,128)(2,1)S(1)} %get-tuple-element.28) | copy-start | bytes 1572868
  304.8 4.0 copy-start.15
  308.8 2.4 copy-start.5
  311.1 2.6 copy-start.3
  311.1 236.5 %reduce-scatter.8.cloned.1.call-start = ((), (), s32[]{:S(2)}) async-start(), calls=%async_computation.9 | async-start | bytes 14155776 | tf_op jit(solution)/shard_map/reduce_scatter | solution.py:112
  311.2 2.5 copy-start.11
  313.7 1.3 copy-start.9
  323.9 1.2 copy-start.6
  323.9 1.6 copy-start.7
  325.1 11.0 %copy-start.13 = (f32[2048]{0:T(1024)S(1)}, f32[2048]{0:T(1024)}, u32[]{:S(2)}) copy-start(f32[2048]{0:T(1024)} %param.14) | copy-start | bytes 24580
  339.4 209.8 %copy-start = (f32[256,1024]{0,1:T(8,128)S(1)}, f32[256,1024]{0,1:T(8,128)}, u32[]{:S(2)}) copy-start(f32[256,1024]{0,1:T(8,128)} %copy.48) | copy-start | bytes 3145732
  551.1 5.2 copy-start.1
Sparse Core Ops, SparseCore 0:
  10.6 25.2 all-gather.4
  38.1 123.7 all-gather.6
  164.0 71.3 all-gather.8
  247.3 29.6 reduce-scatter.9
  283.5 16.6 all-gather.10
  311.2 24.8 reduce-scatter.5
  339.7 207.8 reduce-scatter.7
